TPU v7x, 32 devices: a whole 2x2x4 slice. The times are simulated.
32 devices in a mesh: dp: 4 (over y, x), kv: 4 (over z), tp: 2 (over core).
Axes of the slice: x: 2, y: 2, z: 4, core: 2. Of those that a mesh axis runs over, the one named last changes fastest.
Arguments:
- tokens: bfloat16 [4, 3072, 2048], P('dp', 'kv'), may hold values from -60 to 60
- query_weight: bfloat16 [2048, 1024], P(None, 'tp'), may hold values from -0.125 to 0.125
- key_weight: bfloat16 [2048, 256], P(None, 'tp'), may hold values from -0.125 to 0.125
- value_weight: bfloat16 [2048, 256], P(None, 'tp'), may hold values from -0.125 to 0.125
- out_weight: bfloat16 [1024, 2048], P('tp'), may hold values from -3 to 3
- norm_gain: float32 [2048], P('tp'), may hold values from 0.1 to 1.9
- chosen_owner: int32 [4, 24, 4], P('dp'), may hold values from -1 to 3, as said below
- chosen_part: int32 [4, 24, 4], P('dp'), may hold values from 0 to 11, as said below
Outputs:
- attended: bfloat16 [4, 3072, 2048], P('dp', 'kv', 'tp')
Inputs may be any that keep to these rules, and one draw needn't show every extreme that they name: `chosen_owner`: within a row the indices other than -1 are different. Every named key block lies wholly before its query block's first position. Among the 6 rows of one index of kv, no index is named by more than 6 rows. `chosen_part`: 0 where the owner is -1.
All inputs are finite; a program needn't handle non-finite values.
Results may differ from a plain program's by a relative error of at most 0.014.
The roundings to bfloat16 on the way count: a program that leaves them out, or rounds other values in their place, can miss the bound.
Values may be sent and summed in bfloat16 or wider, within the bound.
A program may use at most 128 MiB of HBM per device.

v0:
```python
import jax
import jax.numpy as jnp
from jax import lax
from jax.sharding import PartitionSpec as P

D = 2048
HEAD_DIM = 64
QUERY_BLOCK = 128
KEY_BLOCK = 64
rope_base = 10000.0
norm_eps = 1e-06


def rotate(head_rows, positions):
    half_dim = head_rows.shape[-1] // 2
    frequency = rope_base ** (-jnp.arange(half_dim, dtype=jnp.float32) / half_dim)
    angles = positions.astype(jnp.float32)[:, None] * frequency
    cosine = jnp.cos(angles)[:, None, :]
    sine_part = jnp.sin(angles)[:, None, :]
    first_half = head_rows[..., :half_dim]
    second_half = head_rows[..., half_dim:]
    return jnp.concatenate(
        [
            first_half * cosine - second_half * sine_part,
            second_half * cosine + first_half * sine_part,
        ],
        axis=-1,
    )


def rank_within(flat_ids):
    entry_count = flat_ids.shape[0]
    same_owner = flat_ids[:, None] == flat_ids[None, :]
    earlier = jnp.arange(entry_count)[None, :] < jnp.arange(entry_count)[:, None]
    return jnp.sum(jnp.logical_and(same_owner, earlier), axis=1)


def body(
    tokens, query_weight, key_weight, value_weight, out_weight, norm_gain, chosen_owner, chosen_part
):
    row_data = tokens[0]
    tok_count = row_data.shape[0]
    devices = lax.axis_size("kv")
    my_index = lax.axis_index("kv")
    positions = my_index * tok_count + jnp.arange(tok_count, dtype=jnp.int32)
    heads_here = query_weight.shape[1] // HEAD_DIM
    kv_here = key_weight.shape[1] // HEAD_DIM
    group_size = heads_here // kv_here
    kv_width = kv_here * HEAD_DIM
    queries = rotate(
        jnp.dot(row_data, query_weight, preferred_element_type=jnp.float32).reshape(
            tok_count, heads_here, HEAD_DIM
        ),
        positions,
    ).astype(jnp.bfloat16)
    key_rows = (
        rotate(
            jnp.dot(row_data, key_weight, preferred_element_type=jnp.float32).reshape(
                tok_count, kv_here, HEAD_DIM
            ),
            positions,
        )
        .astype(jnp.bfloat16)
        .reshape(tok_count, kv_width)
    )
    value_rows = jnp.dot(row_data, value_weight, preferred_element_type=jnp.float32).astype(
        jnp.bfloat16
    )
    per_device = tok_count // KEY_BLOCK
    qblocks = tok_count // QUERY_BLOCK
    chosen_count = chosen_owner.shape[2]
    owner_ids = chosen_owner[0]
    part_ids = chosen_part[0]
    mine_owner = lax.dynamic_slice_in_dim(owner_ids, my_index * qblocks, qblocks, 0).reshape(
        qblocks * chosen_count
    )
    mine_valid = mine_owner >= 0
    key_blocks = key_rows.reshape(per_device, KEY_BLOCK, kv_width)
    value_blocks = value_rows.reshape(per_device, KEY_BLOCK, kv_width)
    every_owner = owner_ids.reshape(devices, qblocks * chosen_count)
    every_part = part_ids.reshape(devices, qblocks * chosen_count)
    every_rank = jax.vmap(rank_within)(every_owner)
    slot_ids = jnp.arange(qblocks, dtype=jnp.int32)
    picked_mask = jnp.logical_and(
        (every_owner == my_index)[:, None, :], every_rank[:, None, :] == slot_ids[None, :, None]
    )
    wanted = jnp.sum(jnp.where(picked_mask, every_part[:, None, :], 0), axis=2)
    send_keys = key_blocks[wanted]
    send_values = value_blocks[wanted]
    got_keys, got_values = (
        lax.all_to_all(send_keys, "kv", split_axis=0, concat_axis=0, tiled=True),
        lax.all_to_all(send_values, "kv", split_axis=0, concat_axis=0, tiled=True),
    )
    slot_index = jnp.where(mine_valid, mine_owner * qblocks + rank_within(mine_owner), 0)
    picked_keys = got_keys.reshape(devices * qblocks, KEY_BLOCK, kv_width)[slot_index]
    picked_values = got_values.reshape(devices * qblocks, KEY_BLOCK, kv_width)[slot_index]
    block_queries = queries.reshape(qblocks, QUERY_BLOCK, kv_here, group_size, HEAD_DIM)
    chosen_keys = picked_keys.reshape(qblocks, chosen_count * KEY_BLOCK, kv_here, HEAD_DIM)
    chosen_values = picked_values.reshape(qblocks, chosen_count * KEY_BLOCK, kv_here, HEAD_DIM)
    all_keys = jnp.concatenate(
        [chosen_keys, key_rows.reshape(qblocks, QUERY_BLOCK, kv_here, HEAD_DIM)], axis=1
    )
    all_values = jnp.concatenate(
        [chosen_values, value_rows.reshape(qblocks, QUERY_BLOCK, kv_here, HEAD_DIM)], axis=1
    )
    key_valid = jnp.broadcast_to(
        mine_valid.reshape(qblocks, chosen_count, 1), (qblocks, chosen_count, KEY_BLOCK)
    ).reshape(qblocks, chosen_count * KEY_BLOCK)
    far_mask = jnp.broadcast_to(
        key_valid[:, None, :], (qblocks, QUERY_BLOCK, chosen_count * KEY_BLOCK)
    )
    lower_mask = jnp.broadcast_to(
        (jnp.arange(QUERY_BLOCK)[:, None] >= jnp.arange(QUERY_BLOCK)[None, :])[None],
        (qblocks, QUERY_BLOCK, QUERY_BLOCK),
    )
    full_mask = jnp.concatenate([far_mask, lower_mask], axis=2)
    scores = jnp.einsum(
        "bqngd,bknd->bngqk", block_queries, all_keys, preferred_element_type=jnp.float32
    ) * HEAD_DIM ** (-0.5)
    scores = jnp.where(full_mask[:, None, None], scores, -jnp.inf)
    row_max = jnp.max(scores, axis=-1, keepdims=True)
    weights = jnp.exp(scores - row_max)
    weights = (weights / jnp.sum(weights, axis=-1, keepdims=True)).astype(jnp.bfloat16)
    mixed_rows = (
        jnp.einsum("bngqk,bknd->bqngd", weights, all_values, preferred_element_type=jnp.float32)
        .astype(jnp.bfloat16)
        .reshape(tok_count, heads_here * HEAD_DIM)
    )
    terms = jnp.dot(mixed_rows, out_weight, preferred_element_type=jnp.float32)
    projected = lax.psum_scatter(
        terms.astype(jnp.bfloat16), "tp", scatter_dimension=1, tiled=True
    ).astype(jnp.float32)
    row_total = lax.psum(jnp.sum(projected * projected, axis=1), "tp")
    scale_rows = lax.rsqrt(row_total / D + norm_eps)
    result = (projected * scale_rows[:, None] * norm_gain[None, :]).astype(jnp.bfloat16)
    return result[None]


def solution(mesh):
    placed = (
        P("dp", "kv", None),
        P(None, "tp"),
        P(None, "tp"),
        P(None, "tp"),
        P("tp", None),
        P("tp"),
        P("dp", None, None),
        P("dp", None, None),
    )
    return jax.shard_map(
        body, mesh=mesh, in_specs=placed, out_specs=P("dp", "kv", "tp"), check_vma=False
    )
```

profile of v0, /device:TPU:0, one launch (start us, length us, event | category | flops | bytes accessed | tf_op | source)
XLA Modules:
  0.0 117.1 jit_solution(5359210719336470150)
XLA Ops:
  7.2 2.3 %copy.52 = bf16[2048,128]{0,1:T(8,128)(2,1)} copy(bf16[2048,128]{1,0:T(8,128)(2,1)} %param.10) | data formatting | bytes 1048576 | tf_op args[2]
  9.9 2.2 %fusion.13 = f32[768,2,64]{0,2,1:T(8,128)S(1)} fusion(bf16[2,64,2048]{2,1,0:T(8,128)(2,1)} %bitcast.97, bf16[1,768,2048]{2,1,0:T(8,128)(2,1)S(1)} %copy-done), kind=kOutput, calls=%fused_computation.22 | convolution fusion | flops 402653184 | bytes 4063232 | tf_op jit(solution)/shard_map/dot_general | solution.py:58
  12.9 1.1 copy.53
  14.0 1.2 %convert_element_type.47 = bf16[12,64,128]{2,1,0:T(8,128)(2,1)S(1)} reshape(bf16[768,2,64]{2,1,0:T(2,128)(2,1)} %copy.53) | data formatting | bytes 393216 | tf_op jit(solution)/shard_map/convert_element_type | solution.py:63
  15.9 1.5 %convert_reduce_fusion = s32[4,24]{1,0:T(4,128)} fusion(s32[4,24]{1,0:T(4,128)S(1)} %reshape_squeeze.3, pred[24,24]{1,0:T(8,128)(4,1)} %iota_compare_fusion.2), kind=kLoop, calls=%fused_computation.49 | loop fusion | flops 9120 | bytes 1344 | tf_op jit(solution)/shard_map/vmap()/reduce_sum | solution.py:35
  19.3 1.4 %gather_fusion.2 = bf16[24,64,128]{2,1,0:T(8,128)(2,1)} fusion(bf16[12,64,128]{2,1,0:T(8,128)(2,1)S(1)} %convert_element_type.47, s32[1024]{0:T(1024)S(1)} %pad_clamp_fusion.1), kind=kCustom, calls=%fused_computation.2 | custom fusion | bytes 786528 | tf_op jit(solution)/shard_map/gather | solution.py:88
  20.7 6.3 %all-to-all-start.1 = ((bf16[4,6,64,128]{3,2,1,0:T(8,128)(2,1)}), bf16[4,6,64,128]{3,2,1,0:T(8,128)(2,1)}, u32[]{:S(2)}, u32[]{:S(2)}) async-start(bf16[4,6,64,128]{3,2,1,0:T(8,128)(2,1)} %bitcast.95), calls=%async_computation.1 | async-start | bytes 786432 | tf_op jit(solution)/shard_map/all_to_all | solution.py:91
  28.9 4.0 %copy.57 = bf16[2048,512]{0,1:T(8,128)(2,1)} copy(bf16[2048,512]{1,0:T(8,128)(2,1)} %param.9) | data formatting | bytes 4194304 | tf_op args[1]
  32.9 4.6 %fusion.11 = f32[768,8,64]{0,2,1:T(8,128)} fusion(bf16[8,64,2048]{2,1,0:T(8,128)(2,1)} %bitcast.92, bf16[1,768,2048]{2,1,0:T(8,128)(2,1)S(1)} %copy-done), kind=kOutput, calls=%fused_computation.20 | convolution fusion | flops 1610612736 | bytes 6815744 | tf_op jit(solution)/shard_map/dot_general | solution.py:51
  37.5 1.0 fusion.20
  38.5 1.3 %gather_fusion = bf16[24,64,128]{2,1,0:T(8,128)(2,1)} fusion(bf16[12,64,128]{2,1,0:T(8,128)(2,1)S(1)} %bitcast.93, s32[1024]{0:T(1024)S(1)} %pad_clamp_fusion.1), kind=kCustom, calls=%fused_computation | custom fusion | bytes 786528 | tf_op jit(solution)/shard_map/gather | solution.py:89
  40.6 2.5 %subtract_convert_fusion = (bf16[768,8,32]{0,2,1:T(8,128)(2,1)}, bf16[768,8,32]{0,2,1:T(8,128)(2,1)}) fusion(f32[768,8,64]{0,2,1:T(8,128)} %fusion.11, f32[768,32]{0,1:T(8,128)S(1)} %get-tuple-element.12, f32[768,32]{0,1:T(8,128)S(1)} %get-tuple-element.11), kind=kLoop, calls=%fused_computation.35 | loop fusion | flops 1572864 | bytes 2555904 | tf_op jit(solution)/shard_map/convert.3
  43.0 5.1 %all-to-all-start = ((bf16[4,6,64,128]{3,2,1,0:T(8,128)(2,1)}), bf16[4,6,64,128]{3,2,1,0:T(8,128)(2,1)}, u32[]{:S(2)}, u32[]{:S(2)}) async-start(bf16[4,6,64,128]{3,2,1,0:T(8,128)(2,1)} %bitcast.94), calls=%async_computation | async-start | bytes 786432 | tf_op jit(solution)/shard_map/all_to_all | solution.py:92
  50.0 2.2 %concatenate.37 = bf16[6,128,2,4,32]{1,0,4,3,2:T(8,128)(2,1)} reshape(bf16[768,8,32]{0,2,1:T(8,128)(2,1)} %get-tuple-element.7) | data formatting | bytes 786432 | tf_op jit(solution)/shard_map/concatenate | solution.py:22
  52.2 1.9 %copy.58 = bf16[6,128,2,4,32]{1,4,3,2,0:T(8,128)(2,1)} copy(bf16[6,128,2,4,32]{1,0,4,3,2:T(8,128)(2,1)} %concatenate.37) | data formatting | bytes 786432 | tf_op jit(solution)/shard_map/concatenate | solution.py:22
  54.1 2.2 %concatenate.38 = bf16[6,128,2,4,32]{1,0,4,3,2:T(8,128)(2,1)} reshape(bf16[768,8,32]{0,2,1:T(8,128)(2,1)} %get-tuple-element.8) | data formatting | bytes 786432 | tf_op jit(solution)/shard_map/concatenate | solution.py:22
  56.3 1.9 %copy.59 = bf16[6,128,2,4,32]{1,4,3,2,0:T(8,128)(2,1)} copy(bf16[6,128,2,4,32]{1,0,4,3,2:T(8,128)(2,1)} %concatenate.38) | data formatting | bytes 786432 | tf_op jit(solution)/shard_map/concatenate | solution.py:22
  58.2 0.9 copy.50
  60.2 1.7 %copy_bitcast_fusion = (bf16[6,128,2,32]{1,3,2,0:T(8,128)(2,1)}, bf16[6,128,2,32]{1,3,2,0:T(8,128)(2,1)}) fusion(bf16[768,2,32]{0,2,1:T(8,128)(2,1)} %copy-done.2, bf16[768,2,32]{0,2,1:T(8,128)(2,1)} %copy-done.3), kind=kLoop, calls=%fused_computation.46 | loop fusion | bytes 393216 | tf_op jit(solution)/shard_map/concatenate | solution.py:22
  61.9 1.6 %gather_fusion.3 = bf16[24,64,128]{2,1,0:T(8,128)(2,1)S(1)} fusion(bf16[24,64,128]{2,1,0:T(8,128)(2,1)} %bitcast.14, s32[1024]{0:T(1024)S(1)} %pad_clamp_fusion), kind=kCustom, calls=%fused_computation.3 | custom fusion | bytes 786528 | tf_op jit(solution)/shard_map/gather | solution.py:95
  63.5 1.2 %reshape.208 = bf16[6,256,2,64]{3,2,1,0:T(2,128)(2,1)} reshape(bf16[24,64,128]{2,1,0:T(8,128)(2,1)S(1)} %gather_fusion.3) | data formatting | bytes 786432 | tf_op jit(solution)/shard_map/reshape | solution.py:98
  64.8 2.9 %copy.56 = bf16[6,256,2,64]{1,3,2,0:T(8,128)(2,1)} copy(bf16[6,256,2,64]{3,2,1,0:T(2,128)(2,1)} %reshape.208) | data formatting | bytes 786432 | tf_op jit(solution)/shard_map/reshape | solution.py:98
  67.6 1.6 %gather_fusion.1 = bf16[24,64,128]{2,1,0:T(8,128)(2,1)S(1)} fusion(bf16[24,64,128]{2,1,0:T(8,128)(2,1)} %bitcast.4, s32[1024]{0:T(1024)S(1)} %pad_clamp_fusion), kind=kCustom, calls=%fused_computation.1 | custom fusion | bytes 786528 | tf_op jit(solution)/shard_map/gather | solution.py:96
  69.2 1.2 %reshape.205 = bf16[6,256,2,64]{3,2,1,0:T(2,128)(2,1)} reshape(bf16[24,64,128]{2,1,0:T(8,128)(2,1)S(1)} %gather_fusion.1) | data formatting | bytes 786432 | tf_op jit(solution)/shard_map/reshape | solution.py:99
  70.5 2.2 %copy.49 = bf16[6,256,2,64]{1,3,2,0:T(8,128)(2,1)S(1)} copy(bf16[6,256,2,64]{3,2,1,0:T(2,128)(2,1)} %reshape.205) | data formatting | bytes 786432 | tf_op jit(solution)/shard_map/reshape | solution.py:99
  72.7 8.9 %fusion.38 = (f32[6,2,4,128]{3,2,1,0:T(4,128)}, f32[6,2,4,128,384]{3,4,2,1,0:T(8,128)}) fusion(pred[6,128,384]{1,2,0:T(8,128)(4,1)} %pad_add_fusion, bf16[6,128,2,4,32]{1,4,3,2,0:T(8,128)(2,1)} %copy.59, bf16[6,128,2,4,32]{1,4,3,2,0:T(8,128)(2,1)} %copy.58, bf16[6,128,2,32]{1,3,2,0:T(8,128)(2,1)} %get-tuple-element.15, ...), kind=kOutput, calls=%fused_computation.74 | convolution fusion | flops 314769792 | bytes 11132928 | tf_op jit(solution)/shard_map/sub | solution.py:122
  81.5 4.8 %fusion.19 = bf16[6,128,2,4,64]{1,4,3,2,0:T(8,128)(2,1)S(1)} fusion(f32[6,2,4,128,384]{3,4,2,1,0:T(8,128)} %get-tuple-element.14, f32[6,2,4,128]{3,2,1,0:T(4,128)} %get-tuple-element.13, bf16[6,128,2,64]{1,3,2,0:T(8,128)(2,1)} %copy.50, bf16[6,256,2,64]{1,3,2,0:T(8,128)(2,1)S(1)} %copy.49), kind=kOutput, calls=%fused_computation.28 | convolution fusion | flops 308281344 | bytes 10838016 | tf_op jit(solution)/shard_map/bngqk,bknd->bqngd/dot_general | solution.py:125
  86.9 3.5 %convolution_convert_fusion = bf16[768,2048]{1,0:T(8,128)(2,1)} fusion(bf16[512,2048]{1,0:T(8,128)(2,1)S(1)} %copy-done.7, bf16[64,8,6,128]{3,2,1,0:T(8,128)(2,1)S(1)} %bitcast.96), kind=kOutput, calls=%fused_computation.16 | convolution fusion | flops 1612185600 | bytes 6029312 | tf_op jit(solution)/shard_map/dot_general | solution.py:129
  90.4 12.6 %reduce-scatter.2.cloned.1.call-done = bf16[768,1024]{1,0:T(8,128)(2,1)} async-done(((bf16[768,2048]{1,0:T(8,128)(2,1)}), bf16[768,1024]{1,0:T(8,128)(2,1)}) %reduce-scatter.2.cloned.1.call-update) | async-done | bytes 1572880 | tf_op jit(solution)/shard_map/reduce_scatter | solution.py:130
  103.0 1.8 %fusion.8 = f32[768]{0:T(1024)S(1)} fusion(bf16[768,1024]{1,0:T(8,128)(2,1)} %reduce-scatter.2.cloned.1.call-done), kind=kLoop, calls=%fused_computation.17 | loop fusion | flops 2358528 | bytes 1575936 | tf_op jit(solution)/shard_map/reduce_sum | solution.py:133
  104.8 2.5 %psum.7 = f32[768]{0:T(1024)S(1)} all-reduce(f32[768]{0:T(1024)S(1)} %fusion.8), channel_id=1, replica_groups=mesh['dp'=4,'kv'=4,'tp'=2] {'tp'}, use_global_device_ids=true, to_apply=%region_7.8 | all-reduce | flops 768 | bytes 6144 | tf_op jit(solution)/shard_map/psum | solution.py:133
  107.3 3.0 %fusion.17 = bf16[1,768,1024]{2,1,0:T(8,128)(2,1)} fusion(bf16[768,1024]{1,0:T(8,128)(2,1)} %reduce-scatter.2.cloned.1.call-done, f32[1024]{0:T(1024)S(1)} %copy-done.5, f32[768]{0:T(1024)S(1)} %add_rsqrt_fusion), kind=kLoop, calls=%fused_computation.26 | loop fusion | flops 3145728 | bytes 3152896 | tf_op jit(solution)/shard_map/broadcast_in_dim | solution.py:136
  (60 shorter events, 10.5 us)
Async XLA Ops:
  6.5 3.4 %copy-start = (bf16[1,768,2048]{2,1,0:T(8,128)(2,1)S(1)}, bf16[1,768,2048]{2,1,0:T(8,128)(2,1)}, u32[]{:S(2)}) copy-start(bf16[1,768,2048]{2,1,0:T(8,128)(2,1)} %param.8) | copy-start | bytes 9437188
  9.9 5.3 %copy-start.4 = (s32[1,24,4]{1,2,0:T(4,128)S(1)}, s32[1,24,4]{1,2,0:T(4,128)}, u32[]{:S(2)}) copy-start(s32[1,24,4]{1,2,0:T(4,128)} %param.14) | copy-start | bytes 1156
  12.2 0.6 copy-start.2
  12.2 0.7 copy-start.3
  20.7 22.3 %all-to-all-start.1 = ((bf16[4,6,64,128]{3,2,1,0:T(8,128)(2,1)}), bf16[4,6,64,128]{3,2,1,0:T(8,128)(2,1)}, u32[]{:S(2)}, u32[]{:S(2)}) async-start(bf16[4,6,64,128]{3,2,1,0:T(8,128)(2,1)} %bitcast.95), calls=%async_computation.1 | async-start | bytes 786432 | tf_op jit(solution)/shard_map/all_to_all | solution.py:91
  32.9 4.6 %copy-start.8 = (bf16[2048,128]{1,0:T(8,128)(2,1)S(1)}, bf16[2048,128]{1,0:T(8,128)(2,1)}, u32[]{:S(2)}) copy-start(bf16[2048,128]{1,0:T(8,128)(2,1)} %param.11) | copy-start | bytes 1572868
  40.6 9.2 %copy-start.6 = (pred[6,4]{0,1:T(4,128)(4,1)S(1)}, pred[6,4]{0,1:T(4,128)(4,1)}, u32[]{:S(2)}) copy-start(pred[6,4]{0,1:T(4,128)(4,1)} %fusion.43) | copy-start | bytes 76
  43.0 24.6 %all-to-all-start = ((bf16[4,6,64,128]{3,2,1,0:T(8,128)(2,1)}), bf16[4,6,64,128]{3,2,1,0:T(8,128)(2,1)}, u32[]{:S(2)}, u32[]{:S(2)}) async-start(bf16[4,6,64,128]{3,2,1,0:T(8,128)(2,1)} %bitcast.94), calls=%async_computation | async-start | bytes 786432 | tf_op jit(solution)/shard_map/all_to_all | solution.py:92
  48.1 54.9 %reduce-scatter.2.cloned.1.call-start = ((), (), s32[]{:S(2)}) async-start(), calls=%async_computation.3 | async-start | bytes 4718592 | tf_op jit(solution)/shard_map/reduce_scatter | solution.py:130
  49.7 8.5 %copy-start.1 = (bf16[6,128,2,64]{3,2,1,0:T(2,128)(2,1)S(1)}, bf16[6,128,2,64]{3,2,1,0:T(2,128)(2,1)}, u32[]{:S(2)}) copy-start(bf16[6,128,2,64]{3,2,1,0:T(2,128)(2,1)} %reshape.247) | copy-start | bytes 589828
  81.5 5.4 %copy-start.7 = (bf16[512,2048]{1,0:T(8,128)(2,1)S(1)}, bf16[512,2048]{1,0:T(8,128)(2,1)}, u32[]{:S(2)}) copy-start(bf16[512,2048]{1,0:T(8,128)(2,1)} %param.12) | copy-start | bytes 6291460
  90.4 16.9 %copy-start.5 = (f32[1024]{0:T(1024)S(1)}, f32[1024]{0:T(1024)}, u32[]{:S(2)}) copy-start(f32[1024]{0:T(1024)} %param.13) | copy-start | bytes 12292
Sparse Core Ops, SparseCore 0:
  90.5 12.3 reduce-scatter.1
where the time goes:
time: 118 us; the launch traced here: 117 us
  local copies, waits for them, and re-layouts  37.9 us (32%)
  matrix products  25 us (21%)
  other arithmetic  14.1 us (12%)
  between operations  13.6 us (12%)
  waiting for transfers between devices  12.6 us (11%)
  starting transfers between devices  11.4 us (10%)
  blocking collectives  2.47 us (2%)
    reduce_scatter x1, waiting for transfers between devices, body(): lax.psum_scatter(terms.astype(jnp.bfloat16), 'tp', scatter_dimension=1, t...  12.6 us
    concatenate x6, local copies, waits for them, and re-layouts, rotate(): jnp.concatenate([first_half * cosine - second_half * sine_part, second_ha...  11 us
    sub x1, matrix products, body(): weights = jnp.exp(scores - row_max)  8.85 us
    unnamed x22, local copies, waits for them, and re-layouts  7.87 us
    all_to_all x1, starting transfers between devices, body(): lax.all_to_all(send_keys, 'kv', split_axis=0, concat_axis=0, tiled=True)  6.35 us
    all_to_all x1, starting transfers between devices, body(): lax.all_to_all(send_values, 'kv', split_axis=0, concat_axis=0, tiled=True)  5.1 us
    dot_general x1, matrix products, body(): jnp.einsum('bngqk,bknd->bqngd', weights, all_values, preferred_element_ty...  4.79 us
    dot_general x1, matrix products, body(): jnp.dot(row_data, query_weight, preferred_element_type=jnp.float32)  4.62 us
  transfers between devices with their start and end apart: 3, of which 1 were waited for; matrix products, arithmetic and copies ran while one was open for 30% of the time, Pallas kernels for 0%

commit v1 on v0

--- a/solution.py
+++ b/solution.py
@@ -1,3 +1,4 @@
+import functools
 import jax
 import jax.numpy as jnp
 from jax import lax
@@ -9,6 +10,39 @@
 KEY_BLOCK = 64
 rope_base = 10000.0
 norm_eps = 1e-06
+
+
+def _recast_ratios(a0, k_dim, v0):
+    v_now = a0.shape
+    tile_out = a0.reshape(*v_now[:k_dim], v0, v_now[k_dim] // v0, *v_now[k_dim + 1 :])
+    high = jnp.moveaxis(tile_out, k_dim, 0)
+    return high
+
+
+def direct_the_region(array_in, array_axis):
+    fresh = list(array_in.shape[1:])
+    fresh[array_axis] *= array_in.shape[0]
+    met_up = jnp.moveaxis(array_in, 0, array_axis).reshape(fresh)
+    return met_up
+
+
+def refer_the_area(xx, ax_name, w_in, x_in):
+    local_out, local_next = (lax.axis_size(ax_name), lax.axis_index(ax_name))
+    part_now = _recast_ratios(xx, w_in, local_out)
+    rows = [part_now[local_next]]
+    for jj in range(1, local_out):
+        back = part_now[(local_next + jj) % local_out]
+        step_out = lax.ppermute(
+            back, ax_name, [(kk, (kk + jj) % local_out) for kk in range(local_out)]
+        )
+        rows.append(step_out)
+    block_out = jnp.stack(rows)
+    part_now = block_out[(local_next - jnp.arange(local_out)) % local_out]
+    carry_in = direct_the_region(part_now, x_in)
+    return carry_in
+
+
+order_layers_all_by_axis = functools.partial(refer_the_area, ax_name="kv", w_in=0, x_in=0)
 
 
 def rotate(head_rows, positions):
@@ -88,7 +122,7 @@
     send_keys = key_blocks[wanted]
     send_values = value_blocks[wanted]
     got_keys, got_values = (
-        lax.all_to_all(send_keys, "kv", split_axis=0, concat_axis=0, tiled=True),
+        order_layers_all_by_axis(send_keys),
         lax.all_to_all(send_values, "kv", split_axis=0, concat_axis=0, tiled=True),
     )
     slot_index = jnp.where(mine_valid, mine_owner * qblocks + rank_within(mine_owner), 0)

time: 118 us -> 125 us (1.059)
  local copies, waits for them, and re-layouts: 37.9 us -> 43.2 us
  other arithmetic: 14.1 us -> 16 us
    ppermute x0 -> x3, starting transfers between devices: none -> 6.99 us  [refer_the_area(): lax.ppermute(back, ax_name, [(kk, (kk + jj) % local_out) for kk in range(...]
    all_to_all x1 -> x0, starting transfers between devices: 6.35 us -> none  [body(): lax.all_to_all(send_keys, 'kv', split_axis=0, concat_axis=0, tiled=True)]
    concatenate x6, local copies, waits for them, and re-layouts: 11 us -> 9.05 us  [rotate(): jnp.concatenate([first_half * cosine - second_half * sine_part, second_ha...]
    dynamic_slice x0 -> x1, local copies, waits for them, and re-layouts: none -> 1.8 us  [refer_the_area(): rows = [part_now[local_next]]]
    gather x0 -> x1, local copies, waits for them, and re-layouts: none -> 1.46 us  [refer_the_area(): part_now = block_out[(local_next - jnp.arange(local_out)) % local_out]]
    gather x0 -> x1, other arithmetic: none -> 1.25 us  [refer_the_area(): part_now = block_out[(local_next - jnp.arange(local_out)) % local_out]]
    another operation x2 -> x3, other arithmetic: 2.51 us -> 2.09 us  [the longest x1 1.09 us: refer_the_area(): block_out = jnp.stack(rows)]
  transfers between devices with their start and end apart: 3 -> 5, of which waited for: 1 -> 1; matrix products, arithmetic and copies ran while one was open for 30% -> 40% of each run, Pallas kernels for 0% -> 0%
where the time goes in v1:
time: 125 us; the launch traced here: 124 us
  local copies, waits for them, and re-layouts  43.2 us (35%)
  matrix products  24.8 us (20%)
  other arithmetic  16 us (13%)
  between operations  13.7 us (11%)
  waiting for transfers between devices  12.3 us (10%)
  starting transfers between devices  11.3 us (9%)
  blocking collectives  2.47 us (2%)
    reduce_scatter x1, waiting for transfers between devices, body(): lax.psum_scatter(terms.astype(jnp.bfloat16), 'tp', scatter_dimension=1, t...  12.3 us
    concatenate x6, local copies, waits for them, and re-layouts, rotate(): jnp.concatenate([first_half * cosine - second_half * sine_part, second_ha...  9.05 us
    sub x1, matrix products, body(): weights = jnp.exp(scores - row_max)  8.71 us
    unnamed x22, local copies, waits for them, and re-layouts  7.19 us
    ppermute x3, starting transfers between devices, refer_the_area(): lax.ppermute(back, ax_name, [(kk, (kk + jj) % local_out) for kk in range(...  6.99 us
    dot_general x1, matrix products, body(): jnp.einsum('bngqk,bknd->bqngd', weights, all_values, preferred_element_ty...  4.8 us
    all_to_all x1, starting transfers between devices, body(): lax.all_to_all(send_values, 'kv', split_axis=0, concat_axis=0, tiled=True)  4.12 us
    dot_general x1, matrix products, body(): terms = jnp.dot(mixed_rows, out_weight, preferred_element_type=jnp.float32)  3.51 us
  transfers between devices with their start and end apart: 5, of which 1 were waited for; matrix products, arithmetic and copies ran while one was open for 40% of the time, Pallas kernels for 0%

profile of v1, /device:TPU:0, one launch (start us, length us, event | category | flops | bytes accessed | tf_op | source)
XLA Modules:
  0.0 123.7 jit_solution(12304263627782367495)
XLA Ops:
  7.2 2.3 %copy.54 = bf16[2048,128]{0,1:T(8,128)(2,1)} copy(bf16[2048,128]{1,0:T(8,128)(2,1)} %param.10) | data formatting | bytes 1048576 | tf_op args[2]
  10.0 2.3 %fusion.13 = f32[768,2,64]{0,2,1:T(8,128)S(1)} fusion(bf16[2,64,2048]{2,1,0:T(8,128)(2,1)} %bitcast.107, bf16[1,768,2048]{2,1,0:T(8,128)(2,1)S(1)} %copy-done), kind=kOutput, calls=%fused_computation.23 | convolution fusion | flops 402653184 | bytes 4063232 | tf_op jit(solution)/shard_map/dot_general | solution.py:92
  15.4 1.5 %convert_reduce_fusion = s32[4,24]{1,0:T(4,128)} fusion(s32[4,24]{1,0:T(4,128)S(1)} %reshape_squeeze.3, pred[24,24]{1,0:T(8,128)(4,1)} %iota_compare_fusion.2), kind=kLoop, calls=%fused_computation.52 | loop fusion | flops 9120 | bytes 1344 | tf_op jit(solution)/shard_map/vmap()/reduce_sum | solution.py:69
  18.8 1.4 %gather_fusion.2 = bf16[24,64,128]{2,1,0:T(8,128)(2,1)} fusion(bf16[12,64,128]{2,1,0:T(8,128)(2,1)S(1)} %convert_element_type.47, s32[1024]{0:T(1024)S(1)} %pad_clamp_fusion.2), kind=kCustom, calls=%fused_computation.2 | custom fusion | bytes 786528 | tf_op jit(solution)/shard_map/gather | solution.py:122
  20.1 1.8 %dynamic-slice_bitcast_fusion = (bf16[1,1,6,64,128]{4,3,2,1,0:T(8,128)(2,1)}, bf16[1,6,64,128]{3,2,1,0:T(8,128)(2,1)}, bf16[1,6,64,128]{3,2,1,0:T(8,128)(2,1)}, bf16[1,6,64,128]{3,2,1,0:T(8,128)(2,1)}) fusion(bf16[4,6,64,128]{3,2,1,0:T(8,128)(2,1)} %bitcast.104, s32[]{:T(128)S(6)} %select_n.99, s32[]{:T(128)S(6)} %select_n.103, s32[]{:T(128)S(6)} %select_n.101, ...), kind=kLoop, calls=%fused_computation.50 | loop fusion | bytes 786448 | tf_op jit(solution)/shard_map/dynamic_slice | solution.py:32
  21.9 3.1 %collective-permute-start = (bf16[1,6,64,128]{3,2,1,0:T(8,128)(2,1)}, bf16[1,6,64,128]{3,2,1,0:T(8,128)(2,1)}, u32[]{:S(2)}, u32[]{:S(2)}) collective-permute-start(bf16[1,6,64,128]{3,2,1,0:T(8,128)(2,1)} %get-tuple-element.13), channel_id=1, source_target_pairs={{0,2},{2,4},{4,6},{6,0},{1,3},{3,5},{5,7},{7,1},{8,10},{10,12},{12... | collective-permute-start | bytes 294920 | tf_op jit(solution)/shard_map/ppermute | solution.py:35
  25.0 2.6 %collective-permute-start.1 = (bf16[1,6,64,128]{3,2,1,0:T(8,128)(2,1)}, bf16[1,6,64,128]{3,2,1,0:T(8,128)(2,1)}, u32[]{:S(2)}, u32[]{:S(2)}) collective-permute-start(bf16[1,6,64,128]{3,2,1,0:T(8,128)(2,1)} %get-tuple-element.12), channel_id=1, source_target_pairs={{0,4},{2,6},{4,0},{6,2},{1,5},{3,7},{5,1},{7,3},{8,12},{10,14},{12... | collective-permute-start | bytes 294920 | tf_op jit(solution)/shard_map/ppermute | solution.py:35
  27.6 1.3 %collective-permute-start.2 = (bf16[1,6,64,128]{3,2,1,0:T(8,128)(2,1)}, bf16[1,6,64,128]{3,2,1,0:T(8,128)(2,1)}, u32[]{:S(2)}, u32[]{:S(2)}) collective-permute-start(bf16[1,6,64,128]{3,2,1,0:T(8,128)(2,1)} %get-tuple-element.14), channel_id=1, source_target_pairs={{0,6},{2,0},{4,2},{6,4},{1,7},{3,1},{5,3},{7,5},{8,14},{10,8},{12,... | collective-permute-start | bytes 294920 | tf_op jit(solution)/shard_map/ppermute | solution.py:35
  28.9 2.0 %fusion.20 = bf16[768,128]{1,0:T(8,128)(2,1)S(1)} fusion(bf16[2048,128]{1,0:T(8,128)(2,1)} %param.11, bf16[1,768,2048]{2,1,0:T(8,128)(2,1)S(1)} %copy-done), kind=kOutput, calls=%fused_computation.31 | convolution fusion | flops 402751488 | bytes 3866624 | tf_op jit(solution)/shard_map/dot_general | solution.py:100
  30.9 1.4 %gather_fusion = bf16[24,64,128]{2,1,0:T(8,128)(2,1)} fusion(bf16[12,64,128]{2,1,0:T(8,128)(2,1)S(1)} %bitcast.102, s32[1024]{0:T(1024)S(1)} %pad_clamp_fusion.2), kind=kCustom, calls=%fused_computation | custom fusion | bytes 786528 | tf_op jit(solution)/shard_map/gather | solution.py:123
  32.3 4.1 %all-to-all-start = ((bf16[4,6,64,128]{3,2,1,0:T(8,128)(2,1)}), bf16[4,6,64,128]{3,2,1,0:T(8,128)(2,1)}, u32[]{:S(2)}, u32[]{:S(2)}) async-start(bf16[4,6,64,128]{3,2,1,0:T(8,128)(2,1)} %bitcast.103), calls=%async_computation | async-start | bytes 786432 | tf_op jit(solution)/shard_map/all_to_all | solution.py:126
  40.8 1.3 %pad_clamp_fusion = s32[1024]{0:T(1024)} fusion(s32[4]{0:T(128)} %fusion.31), kind=kLoop, calls=%fused_computation.59 | loop fusion | flops 1024 | bytes 4112 | tf_op jit(solution)/shard_map/gather | solution.py:40
  47.2 4.0 %copy.59 = bf16[2048,512]{0,1:T(8,128)(2,1)} copy(bf16[2048,512]{1,0:T(8,128)(2,1)} %param.9) | data formatting | bytes 4194304 | tf_op args[1]
  51.1 3.5 %fusion.11 = f32[768,8,64]{0,2,1:T(8,128)S(1)} fusion(bf16[8,64,2048]{2,1,0:T(8,128)(2,1)} %bitcast.101, bf16[1,768,2048]{2,1,0:T(8,128)(2,1)S(1)} %copy-done), kind=kOutput, calls=%fused_computation.21 | convolution fusion | flops 1610612736 | bytes 6815744 | tf_op jit(solution)/shard_map/dot_general | solution.py:85
  55.6 2.2 %concatenate.37 = bf16[6,128,2,4,32]{1,0,4,3,2:T(8,128)(2,1)} reshape(bf16[768,8,32]{0,2,1:T(8,128)(2,1)} %get-tuple-element.7) | data formatting | bytes 786432 | tf_op jit(solution)/shard_map/concatenate | solution.py:56
  57.8 1.9 %copy.60 = bf16[6,128,2,4,32]{1,4,3,2,0:T(8,128)(2,1)} copy(bf16[6,128,2,4,32]{1,0,4,3,2:T(8,128)(2,1)} %concatenate.37) | data formatting | bytes 786432 | tf_op jit(solution)/shard_map/concatenate | solution.py:56
  59.7 1.2 %concatenate.38 = bf16[6,128,2,4,32]{1,0,4,3,2:T(8,128)(2,1)} reshape(bf16[768,8,32]{0,2,1:T(8,128)(2,1)S(1)} %get-tuple-element.8) | data formatting | bytes 786432 | tf_op jit(solution)/shard_map/concatenate | solution.py:56
  60.9 1.9 %copy.61 = bf16[6,128,2,4,32]{1,4,3,2,0:T(8,128)(2,1)} copy(bf16[6,128,2,4,32]{1,0,4,3,2:T(8,128)(2,1)} %concatenate.38) | data formatting | bytes 786432 | tf_op jit(solution)/shard_map/concatenate | solution.py:56
  62.8 1.8 %copy.52 = bf16[6,128,2,64]{1,3,2,0:T(8,128)(2,1)} copy(bf16[6,128,2,64]{3,2,1,0:T(2,128)(2,1)} %reshape.311) | data formatting | bytes 393216 | tf_op jit(solution)/shard_map/reshape | solution.py:138
  68.1 1.5 %gather_fusion.3 = bf16[4,6,64,128]{3,2,1,0:T(8,128)(2,1)} fusion(bf16[4,6,64,128]{3,2,1,0:T(8,128)(2,1)S(1)} %maximum_bitcast_fusion.3, s32[1024]{0:T(1024)} %pad_clamp_fusion), kind=kCustom, calls=%fused_computation.3 | custom fusion | bytes 786448 | tf_op jit(solution)/shard_map/gather | solution.py:40
  69.6 1.6 %gather_fusion.4 = bf16[24,64,128]{2,1,0:T(8,128)(2,1)S(1)} fusion(bf16[24,64,128]{2,1,0:T(8,128)(2,1)} %bitcast.105, s32[1024]{0:T(1024)S(1)} %pad_clamp_fusion.1), kind=kCustom, calls=%fused_computation.4 | custom fusion | bytes 786528 | tf_op jit(solution)/shard_map/gather | solution.py:129
  71.2 1.2 reshape.261
  72.4 2.2 %copy.58 = bf16[6,256,2,64]{1,3,2,0:T(8,128)(2,1)S(1)} copy(bf16[6,256,2,64]{3,2,1,0:T(2,128)(2,1)} %reshape.261) | data formatting | bytes 786432 | tf_op jit(solution)/shard_map/reshape | solution.py:132
  74.6 8.7 %fusion.40 = (f32[6,2,4,128]{3,2,1,0:T(4,128)}, f32[6,2,4,128,384]{3,4,2,1,0:T(8,128)}) fusion(pred[6,128,384]{1,2,0:T(8,128)(4,1)} %pad_add_fusion, bf16[6,128,2,4,32]{1,4,3,2,0:T(8,128)(2,1)} %copy.61, bf16[6,128,2,4,32]{1,4,3,2,0:T(8,128)(2,1)} %copy.60, bf16[6,128,2,32]{1,3,2,0:T(8,128)(2,1)} %get-tuple-element.19, ...), kind=kOutput, calls=%fused_computation.87 | convolution fusion | flops 314769792 | bytes 11132928 | tf_op jit(solution)/shard_map/sub | solution.py:156
  83.3 1.6 %gather_fusion.1 = bf16[24,64,128]{2,1,0:T(8,128)(2,1)S(1)} fusion(bf16[24,64,128]{2,1,0:T(8,128)(2,1)} %bitcast.4, s32[1024]{0:T(1024)S(1)} %pad_clamp_fusion.1), kind=kCustom, calls=%fused_computation.1 | custom fusion | bytes 786528 | tf_op jit(solution)/shard_map/gather | solution.py:130
  86.2 2.2 %copy.51 = bf16[6,256,2,64]{1,3,2,0:T(8,128)(2,1)S(1)} copy(bf16[6,256,2,64]{3,2,1,0:T(2,128)(2,1)} %reshape.259) | data formatting | bytes 786432 | tf_op jit(solution)/shard_map/reshape | solution.py:133
  88.4 4.8 %fusion.19 = bf16[6,128,2,4,64]{1,4,3,2,0:T(8,128)(2,1)S(1)} fusion(f32[6,2,4,128,384]{3,4,2,1,0:T(8,128)} %get-tuple-element.18, f32[6,2,4,128]{3,2,1,0:T(4,128)} %get-tuple-element.17, bf16[6,128,2,64]{1,3,2,0:T(8,128)(2,1)} %copy.52, bf16[6,256,2,64]{1,3,2,0:T(8,128)(2,1)S(1)} %copy.51), kind=kOutput, calls=%fused_computation.29 | convolution fusion | flops 308281344 | bytes 10838016 | tf_op jit(solution)/shard_map/bngqk,bknd->bqngd/dot_general | solution.py:159
  93.7 3.5 %convolution_convert_fusion = bf16[768,2048]{1,0:T(8,128)(2,1)} fusion(bf16[512,2048]{1,0:T(8,128)(2,1)S(1)} %copy-done.8, bf16[64,8,6,128]{3,2,1,0:T(8,128)(2,1)S(1)} %bitcast.106), kind=kOutput, calls=%fused_computation.17 | convolution fusion | flops 1612185600 | bytes 6029312 | tf_op jit(solution)/shard_map/dot_general | solution.py:163
  97.3 12.3 %reduce-scatter.2.cloned.1.call-done = bf16[768,1024]{1,0:T(8,128)(2,1)} async-done(((bf16[768,2048]{1,0:T(8,128)(2,1)}), bf16[768,1024]{1,0:T(8,128)(2,1)}) %reduce-scatter.2.cloned.1.call-update) | async-done | bytes 1572880 | tf_op jit(solution)/shard_map/reduce_scatter | solution.py:164
  109.6 1.8 %fusion.8 = f32[768]{0:T(1024)S(1)} fusion(bf16[768,1024]{1,0:T(8,128)(2,1)} %reduce-scatter.2.cloned.1.call-done), kind=kLoop, calls=%fused_computation.18 | loop fusion | flops 2358528 | bytes 1575936 | tf_op jit(solution)/shard_map/reduce_sum | solution.py:167
  111.4 2.5 %psum.7 = f32[768]{0:T(1024)S(1)} all-reduce(f32[768]{0:T(1024)S(1)} %fusion.8), channel_id=1, replica_groups=mesh['dp'=4,'kv'=4,'tp'=2] {'tp'}, use_global_device_ids=true, to_apply=%region_7.8 | all-reduce | flops 768 | bytes 6144 | tf_op jit(solution)/shard_map/psum | solution.py:167
  113.9 3.0 %fusion.17 = bf16[1,768,1024]{2,1,0:T(8,128)(2,1)} fusion(bf16[768,1024]{1,0:T(8,128)(2,1)} %reduce-scatter.2.cloned.1.call-done, f32[1024]{0:T(1024)S(1)} %copy-done.7, f32[768]{0:T(1024)S(1)} %add_rsqrt_fusion), kind=kLoop, calls=%fused_computation.27 | loop fusion | flops 3145728 | bytes 3152896 | tf_op jit(solution)/shard_map/broadcast_in_dim | solution.py:170
  (69 shorter events, 21.7 us)
Async XLA Ops:
  6.5 3.4 %copy-start = (bf16[1,768,2048]{2,1,0:T(8,128)(2,1)S(1)}, bf16[1,768,2048]{2,1,0:T(8,128)(2,1)}, u32[]{:S(2)}) copy-start(bf16[1,768,2048]{2,1,0:T(8,128)(2,1)} %param.8) | copy-start | bytes 9437188
  9.9 2.3 %copy-start.1 = (f32[768,32]{0,1:T(8,128)}, f32[768,32]{0,1:T(8,128)S(1)}, u32[]{:S(2)}) copy-start(f32[768,32]{0,1:T(8,128)S(1)} %get-tuple-element.15) | copy-start | bytes 294916
  9.9 2.3 %copy-start.3 = (f32[768,32]{0,1:T(8,128)}, f32[768,32]{0,1:T(8,128)S(1)}, u32[]{:S(2)}) copy-start(f32[768,32]{0,1:T(8,128)S(1)} %get-tuple-element.16) | copy-start | bytes 294916
  9.9 4.7 %copy-start.5 = (s32[1,24,4]{1,2,0:T(4,128)S(1)}, s32[1,24,4]{1,2,0:T(4,128)}, u32[]{:S(2)}) copy-start(s32[1,24,4]{1,2,0:T(4,128)} %param.14) | copy-start | bytes 1156
  21.9 45.1 %collective-permute-start = (bf16[1,6,64,128]{3,2,1,0:T(8,128)(2,1)}, bf16[1,6,64,128]{3,2,1,0:T(8,128)(2,1)}, u32[]{:S(2)}, u32[]{:S(2)}) collective-permute-start(bf16[1,6,64,128]{3,2,1,0:T(8,128)(2,1)} %get-tuple-element.13), channel_id=1, source_target_pairs={{0,2},{2,4},{4,6},{6,0},{1,3},{3,5},{5,7},{7,1},{8,10},{10,12},{12... | collective-permute-start | bytes 294920 | tf_op jit(solution)/shard_map/ppermute | solution.py:35
  25.0 42.0 %collective-permute-start.1 = (bf16[1,6,64,128]{3,2,1,0:T(8,128)(2,1)}, bf16[1,6,64,128]{3,2,1,0:T(8,128)(2,1)}, u32[]{:S(2)}, u32[]{:S(2)}) collective-permute-start(bf16[1,6,64,128]{3,2,1,0:T(8,128)(2,1)} %get-tuple-element.12), channel_id=1, source_target_pairs={{0,4},{2,6},{4,0},{6,2},{1,5},{3,7},{5,1},{7,3},{8,12},{10,14},{12... | collective-permute-start | bytes 294920 | tf_op jit(solution)/shard_map/ppermute | solution.py:35
  27.6 9.7 %copy-start.6 = (s32[1,24,4]{1,2,0:T(4,128)S(1)}, s32[1,24,4]{1,2,0:T(4,128)}, u32[]{:S(2)}) copy-start(s32[1,24,4]{1,2,0:T(4,128)} %param.14) | copy-start | bytes 1156
  27.6 39.5 %collective-permute-start.2 = (bf16[1,6,64,128]{3,2,1,0:T(8,128)(2,1)}, bf16[1,6,64,128]{3,2,1,0:T(8,128)(2,1)}, u32[]{:S(2)}, u32[]{:S(2)}) collective-permute-start(bf16[1,6,64,128]{3,2,1,0:T(8,128)(2,1)} %get-tuple-element.14), channel_id=1, source_target_pairs={{0,6},{2,0},{4,2},{6,4},{1,7},{3,1},{5,3},{7,5},{8,14},{10,8},{12,... | collective-permute-start | bytes 294920 | tf_op jit(solution)/shard_map/ppermute | solution.py:35
  32.3 51.0 %all-to-all-start = ((bf16[4,6,64,128]{3,2,1,0:T(8,128)(2,1)}), bf16[4,6,64,128]{3,2,1,0:T(8,128)(2,1)}, u32[]{:S(2)}, u32[]{:S(2)}) async-start(bf16[4,6,64,128]{3,2,1,0:T(8,128)(2,1)} %bitcast.103), calls=%async_computation | async-start | bytes 786432 | tf_op jit(solution)/shard_map/all_to_all | solution.py:126
  36.4 73.2 %reduce-scatter.2.cloned.1.call-start = ((), (), s32[]{:S(2)}) async-start(), calls=%async_computation.2 | async-start | bytes 4718592 | tf_op jit(solution)/shard_map/reduce_scatter | solution.py:164
  51.1 3.5 %copy-start.2 = (f32[768,32]{0,1:T(8,128)S(1)}, f32[768,32]{0,1:T(8,128)}, u32[]{:S(2)}) copy-start(f32[768,32]{0,1:T(8,128)} %copy-done.1) | copy-start | bytes 294916
  51.1 3.5 %copy-start.4 = (f32[768,32]{0,1:T(8,128)S(1)}, f32[768,32]{0,1:T(8,128)}, u32[]{:S(2)}) copy-start(f32[768,32]{0,1:T(8,128)} %copy-done.3) | copy-start | bytes 294916
  88.4 5.4 %copy-start.8 = (bf16[512,2048]{1,0:T(8,128)(2,1)S(1)}, bf16[512,2048]{1,0:T(8,128)(2,1)}, u32[]{:S(2)}) copy-start(bf16[512,2048]{1,0:T(8,128)(2,1)} %param.12) | copy-start | bytes 6291460
  97.3 16.6 %copy-start.7 = (f32[1024]{0:T(1024)S(1)}, f32[1024]{0:T(1024)}, u32[]{:S(2)}) copy-start(f32[1024]{0:T(1024)} %param.13) | copy-start | bytes 12292
Sparse Core Ops, SparseCore 0:
  97.4 12.1 reduce-scatter.1
